TPU v7x, 32 devices: a whole 2x2x4 slice. The times are simulated.
32 devices in a mesh: sp: 8 (over z, y), tp: 4 (over x, core).
Axes of the slice: x: 2, y: 2, z: 4, core: 2. Of those that a mesh axis runs over, the one named last changes fastest.
Arguments:
- tokens: bfloat16 [2048, 2048], P('sp', 'tp'), may hold values from -19 to 250
- in_gain: bfloat16 [2048], replicated, may hold values from 0.099609375 to 1.8984375
- w_glu_value: bfloat16 [2048, 512], P(None, 'tp'), may hold values from -0.125 to 0.125
- w_glu_gate: bfloat16 [2048, 512], P(None, 'tp'), may hold values from -0.125 to 0.125
- w_query: bfloat16 [2048, 1024], P(None, 'tp'), may hold values from -1 to 1
- w_key: bfloat16 [2048, 512], P(None, 'tp'), may hold values from -1 to 1
- w_value: bfloat16 [2048, 512], P(None, 'tp'), may hold values from -0.125 to 0.125
- w_gate_conv: bfloat16 [2048, 512], P(None, 'tp'), may hold values from -0.125 to 0.125
- w_gate_attn: bfloat16 [2048, 1024], P(None, 'tp'), may hold values from -0.125 to 0.125
- conv_weight: bfloat16 [31, 512], P(None, 'tp'), may hold values from -4.6 to 4.6
- conv_gain: float32 [512], P('tp'), may hold values from 0.1 to 1.9
- lam: float32 [8], P('tp'), may hold values from 0.3 to 0.8
- head_gain: float32 [128], replicated, may hold values from 0.1 to 1.9
- out_conv: bfloat16 [512, 2048], P('tp'), may hold values from -0.15625 to 0.15625
- out_attn: bfloat16 [1024, 2048], P('tp'), may hold values from -0.15625 to 0.15625
Outputs:
- mixed: bfloat16 [2048, 2048], P(('sp', 'tp'))
All inputs are finite; a program needn't handle non-finite values.
Results may differ from a plain program's by a relative error of at most 0.017.
The roundings to bfloat16 on the way count: a program that leaves them out, or rounds other values in their place, can miss the bound.
Values may be sent and summed in bfloat16 or wider, within the bound.
A program may use at most 128 MiB of HBM per device.

v0:
```python
import functools
import math

import jax
import jax.numpy as jnp
from jax import lax
from jax.experimental import pallas as pl
from jax.experimental.pallas import tpu as pltpu
from jax.sharding import PartitionSpec as P

EPSILON = 1e-06
NEG_BIG = -1e30
HEAD_SCALE = 0.8
QK = 64
VDIM = 128
MESH = pl.DeviceIdType.MESH
F32 = jnp.float32
BF16 = jnp.bfloat16
PIECES = 4
PAD = 32
LANES = 128
CHUNKS = 2


def dot(a, b, ca=1, cb=0, precision=None):
    return lax.dot_general(
        a, b, (((ca,), (cb,)), ((), ())), preferred_element_type=F32, precision=precision
    )


def kernel(
    n_sp,
    n_tp,
    tok_hbm,
    gain_hbm,
    w_glu_value,
    w_glu_gate,
    w_query,
    w_key,
    w_value,
    w_gate_conv,
    w_gate_attn,
    taps_hbm,
    conv_gain_hbm,
    lam_hbm,
    head_gain_hbm,
    out_conv,
    out_attn,
    out,
    w_all,
    w_out,
    tokbuf,
    acc,
    kbuf,
    vbuf,
    q4,
    m_ref,
    l_ref,
    o_ref,
    gl,
    tail_out,
    tail_in,
    sq_out,
    sq_in,
    ybuf,
    a_out,
    a_own,
    a_in,
    x_out,
    x_in,
    b_out,
    b_own,
    b_in,
    w_sem,
    tok_send,
    tok_recv,
    kv_recv,
    up_send,
    side_send,
    tail_sem,
    sq_send,
    sq_recv,
    a_sem,
    x_sem,
    b_sem,
    gain32,
    tok,
    gain,
    taps_ref,
    conv_gain,
    lam,
    head_gain,
    ga,
    small_sem,
):
    rows, depth = tok.shape
    width = depth * n_tp
    s = lax.axis_index("sp")
    t = lax.axis_index("tp")
    core = t % 2
    p1 = t + 1 - 2 * core
    p2 = (t + 2) % n_tp
    p3 = (p1 + 2) % n_tp
    y = s % 2
    z = s // 2
    mate = s + 1 - 2 * y
    has_up = s + 2 < n_sp

    smalls = [
        pltpu.make_async_copy(src, dst, small_sem.at[i])
        for i, (src, dst) in enumerate((
            (tok_hbm, tok), (gain_hbm, gain), (taps_hbm, taps_ref),
            (conv_gain_hbm, conv_gain), (lam_hbm, lam), (head_gain_hbm, head_gain),
        ))
    ]
    for copy in smalls:
        copy.start()
    weights = (w_key, w_value, w_glu_value, w_glu_gate, w_query, w_gate_conv, w_gate_attn)
    spans = []
    at = 0
    loads = []
    for i, w in enumerate(weights):
        cols = w.shape[1]
        spans.append((at, at + cols))
        loads.append(pltpu.make_async_copy(w, w_all.at[:, at : at + cols], w_sem.at[i]))
        at += cols
    total_cols = at
    at = 0
    out_loads = []
    for i, w in enumerate((out_conv, out_attn)):
        r = w.shape[0]
        out_loads.append(
            pltpu.make_async_copy(w, w_out.at[at : at + r, :], w_sem.at[len(weights) + i])
        )
        at += r
    for copy in loads + out_loads:
        copy.start()

    def tp_copy(src, dst, send, recv, to):
        return pltpu.make_async_remote_copy(
            src_ref=src, dst_ref=dst, send_sem=send, recv_sem=recv,
            device_id={"tp": to}, device_id_type=MESH,
        )

    def sp_copy(src, dst, send, recv, to):
        return pltpu.make_async_remote_copy(
            src_ref=src, dst_ref=dst, send_sem=send, recv_sem=recv,
            device_id={"sp": to}, device_id_type=MESH,
        )

    barrier = pltpu.get_barrier_semaphore()
    for peer in (p1, p2, p3):
        pl.semaphore_signal(barrier, inc=1, device_id={"tp": peer}, device_id_type=MESH)
    for by in (-2, -1, 1, 2):
        other = s + by

        @pl.when((other >= 0) & (other < n_sp))
        def _():
            pl.semaphore_signal(barrier, inc=1, device_id={"sp": other}, device_id_type=MESH)

    pl.semaphore_wait(barrier, 3 + jnp.minimum(s, 2) + jnp.minimum(n_sp - 1 - s, 2))

    for copy in smalls:
        copy.wait()

    half = rows // 2
    across = [
        tp_copy(
            tok.at[c * half : (c + 1) * half], tokbuf.at[1, c * half : (c + 1) * half],
            tok_send.at[c], tok_recv.at[c], p2,
        )
        for c in range(2)
    ]
    beside = tp_copy(tok, tokbuf.at[0], tok_send.at[2], tok_recv.at[2], p1)
    passed = [
        tp_copy(
            tokbuf.at[1, c * half : (c + 1) * half], tokbuf.at[2, c * half : (c + 1) * half],
            tok_send.at[3 + c], tok_recv.at[3 + c], p1,
        )
        for c in range(2)
    ]
    for copy in across:
        copy.start()
    beside.start()

    def prepare(x, owner):
        wide = x.astype(F32)
        first = pl.multiple_of(owner * depth, depth)
        lines = depth // LANES
        parts = [
            wide[:, b * LANES : (b + 1) * LANES] * gain32[pl.ds(owner * lines + b, 1), :]
            for b in range(lines)
        ]
        scaled = jnp.concatenate(parts, axis=1).astype(BF16)
        return scaled, jnp.sum(wide * wide, axis=1, keepdims=True), first

    gain32[...] = gain[...].astype(F32)
    scaled, squares, first = prepare(tok[...], t)
    for copy in loads:
        copy.wait()
    acc[...] = dot(scaled, w_all[pl.ds(first, depth), :])
    beside.wait_recv()
    scaled, more, first = prepare(tokbuf[0], p1)
    squares = squares + more
    acc[...] += dot(scaled, w_all[pl.ds(first, depth), :])
    for c in range(2):
        across[c].wait_recv()
        passed[c].start()
    scaled, more, first = prepare(tokbuf[1], p2)
    squares = squares + more
    acc[...] += dot(scaled, w_all[pl.ds(first, depth), :])
    for c in range(2):
        passed[c].wait_recv()
    scaled, more, first = prepare(tokbuf[2], p3)
    squares = squares + more
    inv_rms = lax.rsqrt(squares / width + EPSILON)
    early = spans[3][1]
    acc[:, :early] += dot(scaled, w_all[pl.ds(first, depth), :early])

    def projected(i, lo=0, hi=None):
        hi = rows if hi is None else hi
        a, b = spans[i]
        return (acc[lo:hi, a:b] * inv_rms[lo:hi]).astype(BF16)

    def glue(lo, hi):
        value = projected(2, lo, hi).astype(F32)
        gate = projected(3, lo, hi).astype(F32)
        return (value * jax.nn.sigmoid(gate)).astype(BF16)

    tail_out[...] = glue(rows - PAD, rows)
    tail = sp_copy(tail_out, tail_in, tail_sem.at[0], tail_sem.at[1], s + 1)

    @pl.when(s + 1 < n_sp)
    def _():
        tail.start()

    def chunk(j, c):
        buf = (kbuf, vbuf)[c * 2 // CHUNKS]
        size = buf.shape[1] * 2 // CHUNKS
        lo = (c % (CHUNKS // 2)) * size
        return buf.at[j, lo : lo + size]

    def up(j, c):
        ref = chunk(j, c)
        return sp_copy(ref, ref, up_send.at[j, c], kv_recv.at[j, c], s + 2)

    def side(j, c):
        ref = chunk(j, c)
        return sp_copy(ref, ref, side_send.at[j, c], kv_recv.at[j, c], mate)

    kbuf[s] = projected(0)
    vbuf[s] = jnp.transpose(projected(1).astype(F32)).astype(BF16)
    for c in range(CHUNKS):

        @pl.when(has_up)
        def _():
            up(s, c).start()

        @pl.when(y == 0)
        def _():
            side(s, c).start()

    acc[:, early:] += dot(scaled, w_all[pl.ds(first, depth), early:])
    query = projected(4).astype(F32) * (1.0 / math.sqrt(QK))
    heads = w_query.shape[1] // (2 * QK)
    lane = lax.broadcasted_iota(jnp.int32, (rows, 2 * QK), 1)
    for h in range(heads):
        qh = query[:, h * 2 * QK : (h + 1) * 2 * QK]
        for m in range(2):
            keep = (lane >= m * QK) & (lane < (m + 1) * QK)
            q4[2 * h + m] = jnp.where(keep, qh, 0.0).astype(BF16)
    gl[PAD:, :] = glue(0, rows).astype(F32)

    gate_attn = projected(6).astype(F32)
    ga[...] = gate_attn * jax.nn.sigmoid(gate_attn)

    key_pos = lax.broadcasted_iota(jnp.int32, (rows, rows), 0)
    query_pos = lax.broadcasted_iota(jnp.int32, (rows, rows), 1)
    allowed = key_pos <= query_pos
    k = kbuf[s]
    v = vbuf[s]
    for i in range(2 * heads):
        scores = jnp.where(allowed, dot(k, q4[i], 1, 1), NEG_BIG)
        top = jnp.max(scores, axis=0, keepdims=True)
        e = jnp.exp(scores - top)
        m_ref[i] = top
        l_ref[i] = jnp.sum(e, axis=0, keepdims=True)
        o_ref[i] = dot(v, e.astype(BF16))

    @pl.when(s == 0)
    def _():
        gl[:PAD, :] = jnp.zeros((PAD, gl.shape[1]), F32)

    @pl.when(s > 0)
    def _():
        tail.wait_recv()
        gl[:PAD, :] = tail_in[...].astype(F32)

    n_taps = taps_ref.shape[0]
    taps = taps_ref[...].astype(F32)
    conv = jnp.zeros((rows, gl.shape[1]), F32)
    for j in range(n_taps):
        lo = PAD - (n_taps - 1) + j
        conv = conv + gl[lo : lo + rows, :] * taps[j : j + 1, :]
    ones = jnp.ones((8, conv.shape[1]), F32)
    high = lax.Precision.HIGHEST
    sq_out[...] = dot(ones, conv * conv, 1, 1, high)
    sq_copies = [
        tp_copy(sq_out, sq_in.at[i], sq_send.at[i], sq_recv.at[i], p)
        for i, p in enumerate((p1, p2, p3))
    ]
    for copy in sq_copies:
        copy.start()

    def visit(j, i, at=slice(None)):
        scores = dot(kbuf[j], q4[i, at, :], 1, 1)
        old = m_ref[i, :, at]
        top = jnp.maximum(old, jnp.max(scores, axis=0, keepdims=True))
        factor = jnp.exp(old - top)
        e = jnp.exp(scores - top)
        m_ref[i, :, at] = top
        l_ref[i, :, at] = l_ref[i, :, at] * factor + jnp.sum(e, axis=0, keepdims=True)
        o_ref[i, :, at] = o_ref[i, :, at] * factor + dot(vbuf[j], e.astype(BF16))

    def mate_arrives(k):
        for c in range(CHUNKS):
            side(mate - 2 * k, c).wait_recv()

    def visit_mate(k, at=slice(None)):
        for i in range(2 * heads):
            visit(mate - 2 * k, i, at)

    maps = 2 * heads // CHUNKS

    def step(i, carry):
        k = i + 1
        j = s - 2 * k
        for c in range(CHUNKS):
            up(j, c).wait_recv()

            @pl.when(has_up)
            def _():
                up(j, c).start()

            side(j, c).start()

            @pl.when(k > 1)
            def _():
                for m in range(maps):
                    visit(j + 2, c * maps + m)

        @pl.when((k > 1) | (y == 1))
        def _():
            mate_arrives(k - 1)
            visit_mate(k - 1)

        return carry

    lax.fori_loop(0, z, step, 0)

    @pl.when(z > 0)
    def _():
        for i in range(2 * heads):
            visit(s - 2 * z, i)

    gate_conv = projected(5).astype(F32)
    for copy in sq_copies:
        copy.wait_recv()
    total_sq = sq_out[...] + sq_in[0] + sq_in[1] + sq_in[2]
    spread = jnp.full((8, conv.shape[1]), 0.125, F32)
    conv_all = conv.shape[1] * n_tp
    mean_sq = dot(total_sq, spread, 0, 0, high) / conv_all
    normed = conv * lax.rsqrt(mean_sq + EPSILON) * conv_gain[...]
    conv_local = conv.shape[1]
    ybuf[:, :conv_local] = (
        normed * jax.nn.sigmoid(normed) * (gate_conv * jax.nn.sigmoid(gate_conv))
    ).astype(BF16)

    part = rows // n_tp
    both = 2 * part
    far_rows = pl.ds(pl.multiple_of(p2 // 2 * both, both), both)
    near_rows = pl.ds(pl.multiple_of(t // 2 * both, both), both)
    more_keys = (z > 0) | (y == 1)

    def finish(at):
        for h in range(heads):
            first_map = o_ref[2 * h, :, at] / l_ref[2 * h, :, at]
            second_map = o_ref[2 * h + 1, :, at] / l_ref[2 * h + 1, :, at]
            o = first_map - lam[:, h : h + 1] * second_map
            n = o * lax.rsqrt(jnp.mean(o * o, axis=0, keepdims=True) + EPSILON)
            n = jnp.transpose(n) * head_gain[...] * HEAD_SCALE
            lo = h * VDIM
            ybuf[at, conv_local + lo : conv_local + lo + VDIM] = (
                n * ga[at, lo : lo + VDIM]
            ).astype(BF16)

    for copy in out_loads:
        copy.wait()

    @pl.when(more_keys)
    def _():
        mate_arrives(z)
        visit_mate(z, far_rows)

    finish(far_rows)


    def block(p):
        return ybuf[pl.ds(pl.multiple_of(p * part, part), part), :]

    cols = w_out.shape[1] // PIECES
    far = jnp.concatenate([block(p3), block(p2)], axis=0)
    a_copies = []
    for c in range(PIECES):
        r = dot(far, w_out[:, c * cols : (c + 1) * cols]).astype(BF16)
        a_out[c] = r[:part]
        a_own[c] = r[part:]
        copy = tp_copy(a_out.at[c], a_in.at[c], a_sem.at[0, c], a_sem.at[1, c], p1)
        copy.start()
        a_copies.append(copy)

    @pl.when(more_keys)
    def _():
        visit_mate(z, near_rows)

    x_copies = []
    for c in range(PIECES):
        a_copies[c].wait_recv()
        x_out[c] = (a_own[c].astype(F32) + a_in[c].astype(F32)).astype(BF16)
        copy = tp_copy(x_out.at[c], x_in.at[c], x_sem.at[0, c], x_sem.at[1, c], p2)
        copy.start()
        x_copies.append(copy)
    finish(near_rows)
    near = jnp.concatenate([block(p1), block(t)], axis=0)
    b_copies = []
    for c in range(PIECES):
        r = dot(near, w_out[:, c * cols : (c + 1) * cols]).astype(BF16)
        b_out[c] = r[:part]
        b_own[c] = r[part:]
        copy = tp_copy(b_out.at[c], b_in.at[c], b_sem.at[0, c], b_sem.at[1, c], p1)
        copy.start()
        b_copies.append(copy)
    for c in range(PIECES):
        b_copies[c].wait_recv()
        x_copies[c].wait_recv()
        out[:, c * cols : (c + 1) * cols] = (
            b_own[c].astype(F32) + b_in[c].astype(F32) + x_in[c].astype(F32)
        ).astype(BF16)

    for copy in across + [beside] + passed + sq_copies + a_copies + x_copies + b_copies:
        copy.wait_send()

    @pl.when(s + 1 < n_sp)
    def _():
        tail.wait_send()

    for c in range(CHUNKS):

        @pl.when(has_up)
        def _():
            up(s, c).wait_send()

        @pl.when(y == 0)
        def _():
            side(s, c).wait_send()

    def drain(i, carry):
        j = s - 2 * (i + 1)
        for c in range(CHUNKS):

            @pl.when(has_up)
            def _():
                up(j, c).wait_send()

            side(j, c).wait_send()
        return carry

    lax.fori_loop(0, z, drain, 0)


def local(n_sp, n_tp, *args):
    (tokens, in_gain, w_glu_value, w_glu_gate, w_query, w_key, w_value, w_gate_conv,
     w_gate_attn, conv_weight, conv_gain, lam, head_gain, out_conv, out_attn) = args
    rows, depth = tokens.shape
    width = depth * n_tp
    weights = (w_glu_value, w_glu_gate, w_query, w_key, w_value, w_gate_conv, w_gate_attn)
    total_cols = sum(w.shape[1] for w in weights)
    out_rows = out_conv.shape[0] + out_attn.shape[0]
    out_cols = out_conv.shape[1]
    conv_local = conv_weight.shape[1]
    heads = lam.shape[0]
    part = rows // n_tp
    cols = out_cols // PIECES
    vmem = pl.BlockSpec(memory_space=pltpu.VMEM)
    hbm = pl.BlockSpec(memory_space=pl.ANY)
    dma = pltpu.SemaphoreType.DMA
    piece = pltpu.VMEM((PIECES, part, cols), BF16)
    return pl.pallas_call(
        functools.partial(kernel, n_sp, n_tp),
        out_shape=jax.ShapeDtypeStruct((part, out_cols), BF16),
        in_specs=[hbm] * len(args),
        out_specs=vmem,
        scratch_shapes=[
            pltpu.VMEM((width, total_cols), BF16),
            pltpu.VMEM((out_rows, out_cols), BF16),
            pltpu.VMEM((3, rows, depth), BF16),
            pltpu.VMEM((rows, total_cols), F32),
            pltpu.VMEM((n_sp, rows, 2 * QK), BF16),
            pltpu.VMEM((n_sp, VDIM, rows), BF16),
            pltpu.VMEM((2 * heads, rows, 2 * QK), BF16),
            pltpu.VMEM((2 * heads, 1, rows), F32),
            pltpu.VMEM((2 * heads, 1, rows), F32),
            pltpu.VMEM((2 * heads, VDIM, rows), F32),
            pltpu.VMEM((PAD + rows, conv_local), F32),
            pltpu.VMEM((PAD, conv_local), BF16),
            pltpu.VMEM((PAD, conv_local), BF16),
            pltpu.VMEM((8, rows), F32),
            pltpu.VMEM((3, 8, rows), F32),
            pltpu.VMEM((rows, out_rows), BF16),
            piece, piece, piece, piece, piece, piece, piece, piece,
            dma((9,)),
            dma((5,)),
            dma((5,)),
            dma((n_sp, CHUNKS)),
            dma((n_sp, CHUNKS)),
            dma((n_sp, CHUNKS)),
            dma((2,)),
            dma((3,)),
            dma((3,)),
            dma((2, PIECES)),
            dma((2, PIECES)),
            dma((2, PIECES)),
            pltpu.VMEM((width // LANES, LANES), F32),
            pltpu.VMEM(tokens.shape, BF16),
            pltpu.VMEM((width // LANES, LANES), BF16),
            pltpu.VMEM(conv_weight.shape, BF16),
            pltpu.VMEM((1, conv_local), F32),
            pltpu.VMEM((1, heads), F32),
            pltpu.VMEM((1, VDIM), F32),
            pltpu.VMEM((rows, heads * VDIM), F32),
            dma((6,)),
        ],
        compiler_params=pltpu.CompilerParams(
            collective_id=0, has_side_effects=True, vmem_limit_bytes=60 * 1024 * 1024
        ),
    )(
        tokens, in_gain.reshape(width // LANES, LANES), w_glu_value, w_glu_gate, w_query, w_key, w_value,
        w_gate_conv, w_gate_attn, conv_weight, conv_gain.reshape(1, conv_local),
        lam.reshape(1, heads),
        head_gain.reshape(1, VDIM), out_conv, out_attn,
    )


def solution(mesh):
    n_sp, n_tp = mesh.shape["sp"], mesh.shape["tp"]
    assert n_tp == 4 and n_sp % 2 == 0
    col = P(None, "tp")
    in_specs = (
        P("sp", "tp"), P(), col, col, col, col, col, col, col, col,
        P("tp"), P("tp"), P(), P("tp", None), P("tp", None),
    )
    return jax.shard_map(
        functools.partial(local, n_sp, n_tp), mesh=mesh, in_specs=in_specs,
        out_specs=P(("sp", "tp"), None), check_vma=False,
    )
```

profile of v0, /device:TPU:25, one launch (start us, length us, event | category | flops | bytes accessed | tf_op | source)
XLA Modules:
  0.0 38.1 jit_solution(7352554549396651467)
XLA Ops:
  0.0 36.4 %shard_map.145 = bf16[64,2048]{1,0:T(8,128)(2,1)} custom-call(bf16[256,512]{1,0:T(8,128)(2,1)} %tok_hbm.1, bf16[16,128]{1,0:T(8,128)(2,1)} %bitcast.4, bf16[2048,128]{1,0:T(8,128)(2,1)} %w_glu_value.1, bf16[2048,128]{1,0:T(8,128)(2,1)} %w_glu_gate.1, bf16[2048,256]{1,0:T(8,128)(2,1)} %w_query.1, bf16[2048,128]{1,0:T(8,128)(2,1)} %w_key.1, ...), custom_call_target="tpu_custom_call" | custom-call | tf_op jit(solution)/shard_map/pallas_call | solution.py:498
  36.4 1.7 %copy.17 = bf16[64,2048]{1,0:T(8,128)(2,1)} copy(bf16[64,2048]{1,0:T(8,128)(2,1)} %shard_map.145) | data formatting | bytes 524288
where the time goes:
time: 38.8 us; the launch traced here: 38.1 us
  Pallas kernels  36.4 us (94%)
  local copies, waits for them, and re-layouts  1.67 us (4%)
    pallas_call x1, Pallas kernels, local(): pl.pallas_call(functools.partial(kernel, n_sp, n_tp), out_shape=jax.Shape...  36.4 us
    unnamed x1, local copies, waits for them, and re-layouts  1.67 us

commit v1 on v0

v1 whole, which is shorter than its diff:
```python
import functools
import math

import jax
import jax.numpy as jnp
from jax import lax
from jax.experimental import pallas as pl
from jax.experimental.pallas import tpu as pltpu
from jax.sharding import PartitionSpec as P

EPSILON = 1e-06
NEG_BIG = -1e30
HEAD_SCALE = 0.8
QK = 64
VDIM = 128
MESH = pl.DeviceIdType.MESH
F32 = jnp.float32
BF16 = jnp.bfloat16
PIECES = 4
PAD = 32
LANES = 128
CHUNKS = 4
NEAR_STEPS = 3
SKIP = 3


def dot(a, b, ca=1, cb=0, precision=None):
    return lax.dot_general(
        a, b, (((ca,), (cb,)), ((), ())), preferred_element_type=F32, precision=precision
    )


def kernel(
    n_sp,
    n_tp,
    tok_hbm,
    gain_hbm,
    w_glu_value,
    w_glu_gate,
    w_query,
    w_key,
    w_value,
    w_gate_conv,
    w_gate_attn,
    taps_hbm,
    conv_gain_hbm,
    lam_hbm,
    head_gain_hbm,
    out_conv,
    out_attn,
    out,
    w_all,
    w_out,
    tokbuf,
    scaled_far,
    acc,
    kv,
    q4,
    m_ref,
    l_ref,
    o_ref,
    gl,
    tail_out,
    tail_in,
    sq_out,
    sq_in,
    ybuf,
    a_out,
    a_own,
    a_in,
    x_out,
    x_in,
    b_out,
    b_own,
    b_in,
    w_sem,
    tok_send,
    tok_recv,
    kv_recv,
    up_send,
    skip_send,
    side_send,
    tail_sem,
    sq_send,
    sq_recv,
    a_sem,
    x_sem,
    b_sem,
    gain32,
    tok,
    gain,
    taps_ref,
    conv_gain,
    lam,
    head_gain,
    ga,
    small_sem,
):
    rows, depth = tok.shape
    width = depth * n_tp
    s = lax.axis_index("sp")
    t = lax.axis_index("tp")
    core = t % 2
    p1 = t + 1 - 2 * core
    p2 = (t + 2) % n_tp
    p3 = (p1 + 2) % n_tp
    y = s % 2
    z = s // 2
    nz = n_sp // 2
    mate = s + 1 - 2 * y
    has_up = s + 2 < n_sp
    has_skip = s + 2 * SKIP < n_sp
    size = rows // CHUNKS
    last_static = min(NEAR_STEPS, nz - 1)

    smalls = [
        pltpu.make_async_copy(src, dst, small_sem.at[i])
        for i, (src, dst) in enumerate((
            (tok_hbm, tok), (gain_hbm, gain), (taps_hbm, taps_ref),
            (conv_gain_hbm, conv_gain), (lam_hbm, lam), (head_gain_hbm, head_gain),
        ))
    ]
    for copy in smalls:
        copy.start()
    weights = (w_key, w_value, w_glu_value, w_glu_gate, w_query, w_gate_conv, w_gate_attn)
    spans = []
    at = 0
    loads = []
    for i, w in enumerate(weights):
        cols = w.shape[1]
        spans.append((at, at + cols))
        loads.append(pltpu.make_async_copy(w, w_all.at[:, at : at + cols], w_sem.at[0]))
        at += cols
    at = 0
    out_loads = []
    for i, w in enumerate((out_conv, out_attn)):
        r = w.shape[0]
        out_loads.append(
            pltpu.make_async_copy(w, w_out.at[at : at + r, :], w_sem.at[1])
        )
        at += r

    def tp_copy(src, dst, send, recv, to):
        return pltpu.make_async_remote_copy(
            src_ref=src, dst_ref=dst, send_sem=send, recv_sem=recv,
            device_id={"tp": to}, device_id_type=MESH,
        )

    def sp_copy(src, dst, send, recv, to):
        return pltpu.make_async_remote_copy(
            src_ref=src, dst_ref=dst, send_sem=send, recv_sem=recv,
            device_id={"sp": to}, device_id_type=MESH,
        )

    barrier = pltpu.get_barrier_semaphore()
    for peer in (p1, p2, p3):
        pl.semaphore_signal(barrier, inc=1, device_id={"tp": peer}, device_id_type=MESH)
    expected = jnp.int32(3)
    for by in (1, 2, 2 * SKIP):
        for other in (s - by, s + by):
            valid = (other >= 0) & (other < n_sp)
            expected = expected + valid.astype(jnp.int32)

            @pl.when(valid)
            def _():
                pl.semaphore_signal(barrier, inc=1, device_id={"sp": other}, device_id_type=MESH)

    for copy in smalls:
        copy.wait()
    for copy in loads:
        copy.start()
    pl.semaphore_wait(barrier, expected)

    def piece_rows(q):
        return slice(q * size, (q + 1) * size)

    across = [
        tp_copy(
            tok.at[piece_rows(q)], tokbuf.at[1, piece_rows(q)],
            tok_send.at[0], tok_recv.at[q], p2,
        )
        for q in range(CHUNKS)
    ]
    passed = [
        tp_copy(
            tokbuf.at[1, piece_rows(q)], tokbuf.at[2, piece_rows(q)],
            tok_send.at[1], tok_recv.at[CHUNKS + q], p1,
        )
        for q in range(CHUNKS)
    ]
    beside = tp_copy(tok, tokbuf.at[0], tok_send.at[2], tok_recv.at[2 * CHUNKS], p1)
    for copy in across:
        copy.start()
    beside.start()
    for copy in out_loads:
        copy.start()

    lines = depth // LANES

    def prepare(x, owner):
        wide = x.astype(F32)
        parts = [
            wide[:, b * LANES : (b + 1) * LANES] * gain32[pl.ds(owner * lines + b, 1), :]
            for b in range(lines)
        ]
        scaled = jnp.concatenate(parts, axis=1).astype(BF16)
        return scaled, jnp.sum(wide * wide, axis=1, keepdims=True)

    def w_rows(owner, lo, hi):
        return w_all[pl.ds(pl.multiple_of(owner * depth, depth), depth), lo:hi]

    first_cols = spans[1][1]
    total_cols = spans[-1][1]
    gain32[...] = gain[...].astype(F32)
    scaled_own, squares = prepare(tok[...], t)
    pltpu.make_async_copy(w_all, w_all, w_sem.at[0]).wait()
    beside.wait_recv()
    scaled, more = prepare(tokbuf[0], p1)
    squares = squares + more
    acc[...] = dot(
        jnp.concatenate([scaled_own, scaled], axis=1),
        jnp.concatenate([w_rows(t, 0, total_cols), w_rows(p1, 0, total_cols)], axis=0),
    )

    def late(q):
        at = piece_rows(q)
        lhs = jnp.concatenate([scaled_far[0, at], scaled_far[1, at]], axis=1)
        rhs = jnp.concatenate(
            [w_rows(p2, first_cols, total_cols), w_rows(p3, first_cols, total_cols)], axis=0
        )
        acc[at, first_cols:] += dot(lhs, rhs)

    def chunk(j, q):
        return kv.at[j, :, piece_rows(q), :]

    def up(j, q):
        return sp_copy(chunk(j, q), chunk(j, q), up_send.at[j], kv_recv.at[j, q], s + 2)

    def skip(q):
        return sp_copy(chunk(s, q), chunk(s, q), skip_send.at[0], kv_recv.at[s, q], s + 2 * SKIP)

    def side(j, q):
        return sp_copy(chunk(j, q), chunk(j, q), side_send.at[j], kv_recv.at[j, q], mate)

    def relay(k, q):
        j = s - 2 * k
        up(j, q).wait_recv()
        if isinstance(k, int):
            if k != SKIP - 1:

                @pl.when(has_up)
                def _():
                    up(j, q).start()
        else:

            @pl.when(has_up & (k != SKIP - 1))
            def _():
                up(j, q).start()

        side(j, q).start()

    def due(k, q):
        lag = 2.4 * k if k < SKIP else 3.8
        return 6.9 + 1.4 * q + lag

    pending = sorted(
        ((k, q) for k in range(1, last_static + 1) for q in range(CHUNKS)),
        key=lambda e: due(*e),
    )

    def relays(until):
        while pending and due(*pending[0]) < until:
            k, q = pending.pop(0)

            @pl.when(z >= k)
            def _():
                relay(k, q)

    inv_parts = []
    for q in range(CHUNKS):
        at = piece_rows(q)
        across[q].wait_recv()
        passed[q].start()
        scaled, sq2 = prepare(tokbuf[1, at], p2)
        scaled_far[0, at] = scaled
        part = acc[at, :first_cols] + dot(scaled, w_rows(p2, 0, first_cols))
        if q > 0:
            late(q - 1)
        passed[q].wait_recv()
        scaled, sq3 = prepare(tokbuf[2, at], p3)
        scaled_far[1, at] = scaled
        part = part + dot(scaled, w_rows(p3, 0, first_cols))
        inv = lax.rsqrt((squares[at] + sq2 + sq3) / width + EPSILON)
        inv_parts.append(inv)
        part = (part * inv).astype(BF16)
        kv[s, 0, at] = part[:, : spans[0][1]]
        kv[s, 1, at] = part[:, spans[1][0] :]

        @pl.when(y == 0)
        def _():
            side(s, q).start()

        @pl.when(has_skip)
        def _():
            skip(q).start()

        @pl.when(has_up)
        def _():
            up(s, q).start()

        relays(7.2 + 1.3 * q)
    late(CHUNKS - 1)
    relays(11.8)
    inv_rms = jnp.concatenate(inv_parts, axis=0)

    def projected(i, lo=0, hi=None):
        hi = rows if hi is None else hi
        a, b = spans[i]
        return (acc[lo:hi, a:b] * inv_rms[lo:hi]).astype(BF16)

    def glue(lo, hi):
        value = projected(2, lo, hi).astype(F32)
        gate = projected(3, lo, hi).astype(F32)
        return (value * jax.nn.sigmoid(gate)).astype(BF16)

    tail_out[...] = glue(rows - PAD, rows)
    tail = sp_copy(tail_out, tail_in, tail_sem.at[0], tail_sem.at[1], s + 1)

    @pl.when(s + 1 < n_sp)
    def _():
        tail.start()

    query = projected(4).astype(F32) * (1.0 / math.sqrt(QK))
    heads = w_query.shape[1] // (2 * QK)
    maps = 2 * heads
    lane = lax.broadcasted_iota(jnp.int32, (rows, 2 * QK), 1)
    for h in range(heads):
        qh = query[:, h * 2 * QK : (h + 1) * 2 * QK]
        for m in range(2):
            keep = (lane >= m * QK) & (lane < (m + 1) * QK)
            q4[2 * h + m] = jnp.where(keep, qh, 0.0).astype(BF16)
    relays(12.6)

    key_pos = lax.broadcasted_iota(jnp.int32, (rows, rows), 0)
    query_pos = lax.broadcasted_iota(jnp.int32, (rows, rows), 1)
    allowed = key_pos <= query_pos
    k_own = kv[s, 0]
    v_own = kv[s, 1]
    scores = [jnp.where(allowed, dot(k_own, q4[i], 1, 1), NEG_BIG) for i in range(maps)]
    tops = [jnp.max(x, axis=0, keepdims=True) for x in scores]
    exps = [jnp.exp(x - top) for x, top in zip(scores, tops)]
    for i in range(maps):
        m_ref[i] = tops[i]
        l_ref[i] = jnp.sum(exps[i], axis=0, keepdims=True)
        o_ref[i] = dot(v_own, exps[i].astype(BF16), 0, 0)
    relays(13.6)

    gl[PAD:, :] = glue(0, rows).astype(F32)
    gate_attn = projected(6).astype(F32)
    ga[...] = gate_attn * jax.nn.sigmoid(gate_attn)

    def visit(blocks, at=slice(None)):
        def stacked(plane):
            parts = [kv[j, plane] for j in blocks]
            return parts[0] if len(parts) == 1 else jnp.concatenate(parts, axis=0)

        k = stacked(0)
        v = stacked(1)
        scores = [dot(k, q4[i, at, :], 1, 1) for i in range(maps)]
        olds = [m_ref[i, :, at] for i in range(maps)]
        tops = [
            jnp.maximum(old, jnp.max(x, axis=0, keepdims=True)) for old, x in zip(olds, scores)
        ]
        exps = [jnp.exp(x - top) for x, top in zip(scores, tops)]
        factors = [jnp.exp(old - top) for old, top in zip(olds, tops)]
        news = [dot(v, e.astype(BF16), 0, 0) for e in exps]
        for i in range(maps):
            m_ref[i, :, at] = tops[i]
            l_ref[i, :, at] = l_ref[i, :, at] * factors[i] + jnp.sum(exps[i], axis=0, keepdims=True)
            o_ref[i, :, at] = o_ref[i, :, at] * factors[i] + news[i]

    def mate_arrives(k):
        for q in range(CHUNKS):
            side(mate - 2 * k, q).wait_recv()

    @pl.when(z >= 1)
    def _():
        visit([s - 2])

    relays(14.8)

    @pl.when(s == 0)
    def _():
        gl[:PAD, :] = jnp.zeros((PAD, gl.shape[1]), F32)

    @pl.when(s > 0)
    def _():
        tail.wait_recv()
        gl[:PAD, :] = tail_in[...].astype(F32)

    n_taps = taps_ref.shape[0]
    taps = taps_ref[...].astype(F32)
    conv = jnp.zeros((rows, gl.shape[1]), F32)
    for j in range(n_taps):
        lo = PAD - (n_taps - 1) + j
        conv = conv + gl[lo : lo + rows, :] * taps[j : j + 1, :]
    ones = jnp.ones((8, conv.shape[1]), F32)
    high = lax.Precision.HIGHEST
    sq_out[...] = dot(ones, conv * conv, 1, 1, high)
    gl[PAD:, :] = conv
    sq_copies = [
        tp_copy(sq_out, sq_in.at[i], sq_send.at[0], sq_recv.at[i], p)
        for i, p in enumerate((p1, p2, p3))
    ]
    for copy in sq_copies:
        copy.start()
    relays(15.4)

    @pl.when(y == 1)
    def _():
        mate_arrives(0)

    @pl.when((y == 1) & (z > 0))
    def _():
        visit([mate])

    relays(100.0)

    if last_static >= 2:

        @pl.when(z == 2)
        def _():
            visit([s - 4])

    if last_static >= 3:

        @pl.when(z >= 3)
        def _():
            visit([s - 4, s - 6])

    def beyond(k, carry):
        for q in range(CHUNKS):
            relay(k, q)
        visit([s - 2 * k])
        return carry

    if nz - 1 > NEAR_STEPS:
        lax.fori_loop(NEAR_STEPS + 1, z + 1, beyond, 0)

    gate_conv = projected(5).astype(F32)
    for copy in sq_copies:
        copy.wait_recv()
    total_sq = sq_out[...] + sq_in[0] + sq_in[1] + sq_in[2]
    conv_local = gl.shape[1]
    spread = jnp.full((8, conv_local), 0.125, F32)
    mean_sq = dot(total_sq, spread, 0, 0, high) / (conv_local * n_tp)
    normed = gl[PAD:, :] * lax.rsqrt(mean_sq + EPSILON) * conv_gain[...]
    ybuf[:, :conv_local] = (
        normed * jax.nn.sigmoid(normed) * (gate_conv * jax.nn.sigmoid(gate_conv))
    ).astype(BF16)

    part = rows // n_tp
    both = 2 * part
    far_rows = pl.ds(pl.multiple_of(p2 // 2 * both, both), both)
    near_rows = pl.ds(pl.multiple_of(t // 2 * both, both), both)

    def finish(at):
        for h in range(heads):
            first_map = o_ref[2 * h, :, at] / l_ref[2 * h, :, at]
            second_map = o_ref[2 * h + 1, :, at] / l_ref[2 * h + 1, :, at]
            o = first_map - lam[:, h : h + 1] * second_map
            n = o * lax.rsqrt(jnp.mean(o * o, axis=0, keepdims=True) + EPSILON)
            n = jnp.transpose(n) * head_gain[...] * HEAD_SCALE
            lo = h * VDIM
            ybuf[at, conv_local + lo : conv_local + lo + VDIM] = (
                n * ga[at, lo : lo + VDIM]
            ).astype(BF16)

    pltpu.make_async_copy(w_out, w_out, w_sem.at[1]).wait()

    def beyond_mate(k, carry):
        mate_arrives(k)
        visit([mate - 2 * k])
        return carry

    if nz - 1 > NEAR_STEPS:
        lax.fori_loop(NEAR_STEPS + 1, z + 1, beyond_mate, 0)

    @pl.when(z >= 1)
    def _():
        mate_arrives(1)

    @pl.when(z >= 2)
    def _():
        visit([mate - 2])
        mate_arrives(2)

    if last_static >= 3:

        @pl.when(z >= 3)
        def _():
            mate_arrives(3)

    def last_mate(at):
        @pl.when((z == 0) & (y == 1))
        def _():
            visit([mate], at)

        @pl.when(z == 1)
        def _():
            visit([mate - 2], at)

        if last_static >= 2:

            @pl.when(z == 2)
            def _():
                visit([mate - 4], at)

        if last_static >= 3:

            @pl.when(z >= 3)
            def _():
                visit([mate - 4, mate - 6], at)

    last_mate(far_rows)
    finish(far_rows)

    def block(p):
        return ybuf[pl.ds(pl.multiple_of(p * part, part), part), :]

    cols = w_out.shape[1] // PIECES
    far = jnp.concatenate([block(p3), block(p2)], axis=0)
    a_copies = []
    for c in range(PIECES):
        r = dot(far, w_out[:, c * cols : (c + 1) * cols]).astype(BF16)
        a_out[c] = r[:part]
        a_own[c] = r[part:]
        copy = tp_copy(a_out.at[c], a_in.at[c], a_sem.at[0], a_sem.at[1 + c], p1)
        copy.start()
        a_copies.append(copy)
    x_copies = []
    for c in range(PIECES):
        a_copies[c].wait_recv()
        x_out[c] = (a_own[c].astype(F32) + a_in[c].astype(F32)).astype(BF16)
        copy = tp_copy(x_out.at[c], x_in.at[c], x_sem.at[0], x_sem.at[1 + c], p2)
        copy.start()
        x_copies.append(copy)
    last_mate(near_rows)
    finish(near_rows)
    near = jnp.concatenate([block(p1), block(t)], axis=0)
    b_copies = []
    for c in range(PIECES):
        r = dot(near, w_out[:, c * cols : (c + 1) * cols]).astype(BF16)
        b_out[c] = r[:part]
        b_own[c] = r[part:]
        copy = tp_copy(b_out.at[c], b_in.at[c], b_sem.at[0], b_sem.at[1 + c], p1)
        copy.start()
        b_copies.append(copy)
    def sent(ref, sem):
        pltpu.make_async_copy(ref, ref, sem).wait()

    sent(tok, tok_send.at[0])
    sent(tok, tok_send.at[1])
    sent(tok, tok_send.at[2])
    sent(sq_in, sq_send.at[0])
    sent(a_out, a_sem.at[0])

    @pl.when(s + 1 < n_sp)
    def _():
        tail.wait_send()

    @pl.when(has_up)
    def _():
        sent(kv.at[s], up_send.at[s])

    @pl.when(has_skip)
    def _():
        sent(kv.at[s], skip_send.at[0])

    @pl.when(y == 0)
    def _():
        sent(kv.at[s], side_send.at[s])

    def drain(k, carry):
        j = s - 2 * k

        @pl.when(has_up & (k != SKIP - 1))
        def _():
            sent(kv.at[j], up_send.at[j])

        sent(kv.at[j], side_send.at[j])
        return carry

    lax.fori_loop(1, z + 1, drain, 0)
    for c in range(PIECES):
        b_copies[c].wait_recv()
    for c in range(PIECES):
        x_copies[c].wait_recv()
        out[:, c * cols : (c + 1) * cols] = (
            b_own[c].astype(F32) + b_in[c].astype(F32) + x_in[c].astype(F32)
        ).astype(BF16)
    sent(x_out, x_sem.at[0])
    sent(b_out, b_sem.at[0])


def local(n_sp, n_tp, *args):
    (tokens, in_gain, w_glu_value, w_glu_gate, w_query, w_key, w_value, w_gate_conv,
     w_gate_attn, conv_weight, conv_gain, lam, head_gain, out_conv, out_attn) = args
    rows, depth = tokens.shape
    width = depth * n_tp
    weights = (w_glu_value, w_glu_gate, w_query, w_key, w_value, w_gate_conv, w_gate_attn)
    total_cols = sum(w.shape[1] for w in weights)
    out_rows = out_conv.shape[0] + out_attn.shape[0]
    out_cols = out_conv.shape[1]
    conv_local = conv_weight.shape[1]
    heads = lam.shape[0]
    part = rows // n_tp
    cols = out_cols // PIECES
    vmem = pl.BlockSpec(memory_space=pltpu.VMEM)
    hbm = pl.BlockSpec(memory_space=pl.ANY)
    dma = pltpu.SemaphoreType.DMA
    piece = pltpu.VMEM((PIECES, part, cols), BF16)
    return pl.pallas_call(
        functools.partial(kernel, n_sp, n_tp),
        out_shape=pltpu.VMEM((part, out_cols), BF16),
        in_specs=[hbm] * len(args),
        out_specs=vmem,
        scratch_shapes=[
            pltpu.VMEM((width, total_cols), BF16),
            pltpu.VMEM((out_rows, out_cols), BF16),
            pltpu.VMEM((3, rows, depth), BF16),
            pltpu.VMEM((2, rows, depth), BF16),
            pltpu.VMEM((rows, total_cols), F32),
            pltpu.VMEM((n_sp, 2, rows, VDIM), BF16),
            pltpu.VMEM((2 * heads, rows, 2 * QK), BF16),
            pltpu.VMEM((2 * heads, 1, rows), F32),
            pltpu.VMEM((2 * heads, 1, rows), F32),
            pltpu.VMEM((2 * heads, VDIM, rows), F32),
            pltpu.VMEM((PAD + rows, conv_local), F32),
            pltpu.VMEM((PAD, conv_local), BF16),
            pltpu.VMEM((PAD, conv_local), BF16),
            pltpu.VMEM((8, rows), F32),
            pltpu.VMEM((3, 8, rows), F32),
            pltpu.VMEM((rows, out_rows), BF16),
            piece, piece, piece, piece, piece, piece, piece, piece,
            dma((2,)),
            dma((3,)),
            dma((2 * CHUNKS + 1,)),
            dma((n_sp, CHUNKS)),
            dma((n_sp,)),
            dma((1,)),
            dma((n_sp,)),
            dma((2,)),
            dma((1,)),
            dma((3,)),
            dma((1 + PIECES,)),
            dma((1 + PIECES,)),
            dma((1 + PIECES,)),
            pltpu.VMEM((width // LANES, LANES), F32),
            pltpu.VMEM(tokens.shape, BF16),
            pltpu.VMEM((width // LANES, LANES), BF16),
            pltpu.VMEM(conv_weight.shape, BF16),
            pltpu.VMEM((1, conv_local), F32),
            pltpu.VMEM((1, heads), F32),
            pltpu.VMEM((1, VDIM), F32),
            pltpu.VMEM((rows, heads * VDIM), F32),
            dma((6,)),
        ],
        compiler_params=pltpu.CompilerParams(
            collective_id=0, has_side_effects=True, vmem_limit_bytes=60 * 1024 * 1024
        ),
    )(
        tokens, in_gain.reshape(width // LANES, LANES), w_glu_value, w_glu_gate, w_query, w_key, w_value,
        w_gate_conv, w_gate_attn, conv_weight, conv_gain.reshape(1, conv_local),
        lam.reshape(1, heads),
        head_gain.reshape(1, VDIM), out_conv, out_attn,
    )


def solution(mesh):
    n_sp, n_tp = mesh.shape["sp"], mesh.shape["tp"]
    assert n_tp == 4 and n_sp % 2 == 0 and 2 * QK == VDIM
    col = P(None, "tp")
    in_specs = (
        P("sp", "tp"), P(), col, col, col, col, col, col, col, col,
        P("tp"), P("tp"), P(), P("tp", None), P("tp", None),
    )
    return jax.shard_map(
        functools.partial(local, n_sp, n_tp), mesh=mesh, in_specs=in_specs,
        out_specs=P(("sp", "tp"), None), check_vma=False,
    )
```

time: 38.8 us -> 34.3 us (0.88); the launches traced: 38.1 us -> 34.1 us
  Pallas kernels: 36.4 us -> 33.4 us
  local copies, waits for them, and re-layouts: 1.67 us -> 0.71 us
    pallas_call x1, Pallas kernels: 36.4 us -> 33.4 us  [local(): pl.pallas_call(functools.partial(kernel, n_sp, n_tp), out_shape=pltpu.VME...]
    unnamed x1, local copies, waits for them, and re-layouts: 1.67 us -> 0.71 us
where the time goes in v1:
time: 34.3 us; the launch traced here: 34.1 us
  Pallas kernels  33.4 us (97%)
  local copies, waits for them, and re-layouts  0.71 us (2%)
    pallas_call x1, Pallas kernels, local(): pl.pallas_call(functools.partial(kernel, n_sp, n_tp), out_shape=pltpu.VME...  33.4 us
    unnamed x1, local copies, waits for them, and re-layouts  0.71 us

profile of v1, /device:TPU:25, one launch (start us, length us, event | category | flops | bytes accessed | tf_op | source)
XLA Modules:
  0.0 34.1 jit_solution(4439086918198286450)
XLA Ops:
  0.0 33.4 %shard_map.145 = bf16[64,2048]{1,0:T(8,128)(2,1)S(1)} custom-call(bf16[256,512]{1,0:T(8,128)(2,1)} %tok_hbm.1, bf16[16,128]{1,0:T(8,128)(2,1)} %bitcast.4, bf16[2048,128]{1,0:T(8,128)(2,1)} %w_glu_value.1, bf16[2048,128]{1,0:T(8,128)(2,1)} %w_glu_gate.1, bf16[2048,256]{1,0:T(8,128)(2,1)} %w_query.1, bf16[2048,128]{1,0:T(8,128)(2,1)} %w_key.1, ...), custom_call_target="tpu_custom_call" | custom-call | tf_op jit(solution)/shard_map/pallas_call | solution.py:623
  33.4 0.7 %copy.17 = bf16[64,2048]{1,0:T(8,128)(2,1)} copy(bf16[64,2048]{1,0:T(8,128)(2,1)S(1)} %shard_map.145) | data formatting | bytes 524288

commit v2 on v1

--- a/solution.py
+++ b/solution.py
@@ -22,6 +22,7 @@
 CHUNKS = 4
 NEAR_STEPS = 3
 SKIP = 3
+HALF = CHUNKS // 2
 
 
 def dot(a, b, ca=1, cb=0, precision=None):
@@ -77,6 +78,7 @@
     tok_send,
     tok_recv,
     kv_recv,
+    side_recv,
     up_send,
     skip_send,
     side_send,
@@ -95,6 +97,8 @@
     head_gain,
     ga,
     small_sem,
+    near_sem,
+    far_sem,
 ):
     rows, depth = tok.shape
     width = depth * n_tp
@@ -156,7 +160,7 @@
     for peer in (p1, p2, p3):
         pl.semaphore_signal(barrier, inc=1, device_id={"tp": peer}, device_id_type=MESH)
     expected = jnp.int32(3)
-    for by in (1, 2, 2 * SKIP):
+    for by in (1, 2):
         for other in (s - by, s + by):
             valid = (other >= 0) & (other < n_sp)
             expected = expected + valid.astype(jnp.int32)
@@ -177,7 +181,7 @@
     across = [
         tp_copy(
             tok.at[piece_rows(q)], tokbuf.at[1, piece_rows(q)],
-            tok_send.at[0], tok_recv.at[q], p2,
+            tok_send.at[0], tok_recv.at[q], p3,
         )
         for q in range(CHUNKS)
     ]
@@ -195,6 +199,16 @@
     for copy in out_loads:
         copy.start()
 
+    def tell(sem):
+        pl.semaphore_signal(sem, inc=1, device_id={"sp": s - 2}, device_id_type=MESH)
+
+    @pl.when((s >= 2) & has_up)
+    def _():
+        tell(near_sem)
+
+    def sent(ref, sem):
+        pltpu.make_async_copy(ref, ref, sem).wait()
+
     lines = depth // LANES
 
     def prepare(x, owner):
@@ -209,10 +223,18 @@
     def w_rows(owner, lo, hi):
         return w_all[pl.ds(pl.multiple_of(owner * depth, depth), depth), lo:hi]
 
-    first_cols = spans[1][1]
+    first_cols = spans[3][1]
     total_cols = spans[-1][1]
     gain32[...] = gain[...].astype(F32)
     scaled_own, squares = prepare(tok[...], t)
+    @pl.when(s + 4 < n_sp)
+    def _():
+        pl.semaphore_wait(near_sem, 1)
+
+    @pl.when((s >= 2) & (s + 4 < n_sp))
+    def _():
+        tell(far_sem)
+
     pltpu.make_async_copy(w_all, w_all, w_sem.at[0]).wait()
     beside.wait_recv()
     scaled, more = prepare(tokbuf[0], p1)
@@ -226,7 +248,7 @@
         at = piece_rows(q)
         lhs = jnp.concatenate([scaled_far[0, at], scaled_far[1, at]], axis=1)
         rhs = jnp.concatenate(
-            [w_rows(p2, first_cols, total_cols), w_rows(p3, first_cols, total_cols)], axis=0
+            [w_rows(p3, first_cols, total_cols), w_rows(p2, first_cols, total_cols)], axis=0
         )
         acc[at, first_cols:] += dot(lhs, rhs)
 
@@ -234,13 +256,13 @@
         return kv.at[j, :, piece_rows(q), :]
 
     def up(j, q):
-        return sp_copy(chunk(j, q), chunk(j, q), up_send.at[j], kv_recv.at[j, q], s + 2)
+        return sp_copy(chunk(j, q), chunk(j, q), up_send.at[j // 2], kv_recv.at[j // 2, q], s + 2)
 
     def skip(q):
-        return sp_copy(chunk(s, q), chunk(s, q), skip_send.at[0], kv_recv.at[s, q], s + 2 * SKIP)
+        return sp_copy(chunk(s, q), chunk(s, q), skip_send.at[0], kv_recv.at[z, q], s + 2 * SKIP)
 
     def side(j, q):
-        return sp_copy(chunk(j, q), chunk(j, q), side_send.at[j], kv_recv.at[j, q], mate)
+        return sp_copy(chunk(j, q), chunk(j, q), side_send.at[j // 2], side_recv.at[j // 2, q // HALF], mate)
 
     def relay(k, q):
         j = s - 2 * k
@@ -259,76 +281,92 @@
 
         side(j, q).start()
 
-    def due(k, q):
-        lag = 2.4 * k if k < SKIP else 3.8
-        return 6.9 + 1.4 * q + lag
-
-    pending = sorted(
-        ((k, q) for k in range(1, last_static + 1) for q in range(CHUNKS)),
-        key=lambda e: due(*e),
-    )
+    def due(steps, k, q):
+        if k == 1:
+            return 9.9 + 1.3 * q
+        return 11.3 + 1.3 * q if k == SKIP else 14.9 + 0.7 * q
+
+    pending = {
+        steps: sorted(
+            ((k, q) for k in range(1, steps + 1) for q in range(CHUNKS)),
+            key=lambda e: due(steps, *e),
+        )
+        for steps in range(1, last_static + 1)
+    }
 
     def relays(until):
-        while pending and due(*pending[0]) < until:
-            k, q = pending.pop(0)
-
-            @pl.when(z >= k)
+        for steps, queue in pending.items():
+            now = []
+            while queue and due(steps, *queue[0]) < until:
+                now.append(queue.pop(0))
+            if not now:
+                continue
+
+            @pl.when((z == steps) if steps < last_static else (z >= steps))
             def _():
-                relay(k, q)
-
+                for k, q in now:
+                    relay(k, q)
+
+    tail = sp_copy(tail_out, tail_in, tail_sem.at[0], tail_sem.at[1], s + 1)
     inv_parts = []
     for q in range(CHUNKS):
         at = piece_rows(q)
         across[q].wait_recv()
         passed[q].start()
-        scaled, sq2 = prepare(tokbuf[1, at], p2)
+        scaled, sq2 = prepare(tokbuf[1, at], p3)
         scaled_far[0, at] = scaled
-        part = acc[at, :first_cols] + dot(scaled, w_rows(p2, 0, first_cols))
+        part = acc[at, :first_cols] + dot(scaled, w_rows(p3, 0, first_cols))
         if q > 0:
             late(q - 1)
         passed[q].wait_recv()
-        scaled, sq3 = prepare(tokbuf[2, at], p3)
+        scaled, sq3 = prepare(tokbuf[2, at], p2)
         scaled_far[1, at] = scaled
-        part = part + dot(scaled, w_rows(p3, 0, first_cols))
+        part = part + dot(scaled, w_rows(p2, 0, first_cols))
         inv = lax.rsqrt((squares[at] + sq2 + sq3) / width + EPSILON)
         inv_parts.append(inv)
         part = (part * inv).astype(BF16)
+
+        def glue():
+            value = part[:, spans[2][0] : spans[2][1]].astype(F32)
+            gate = part[:, spans[3][0] : spans[3][1]].astype(F32)
+            glued = (value * jax.nn.sigmoid(gate)).astype(BF16)
+            gl[PAD + q * size : PAD + (q + 1) * size, :] = glued.astype(F32)
+            return glued
+
+        if q == CHUNKS - 1:
+            tail_out[...] = glue()[size - PAD :]
+
+            @pl.when(s + 1 < n_sp)
+            def _():
+                tail.start()
+
         kv[s, 0, at] = part[:, : spans[0][1]]
-        kv[s, 1, at] = part[:, spans[1][0] :]
+        kv[s, 1, at] = part[:, spans[1][0] : spans[1][1]]
 
         @pl.when(y == 0)
         def _():
             side(s, q).start()
 
+        @pl.when(has_up)
+        def _():
+            up(s, q).start()
+
         @pl.when(has_skip)
         def _():
+            if q == 0:
+                pl.semaphore_wait(far_sem, 1)
             skip(q).start()
 
-        @pl.when(has_up)
-        def _():
-            up(s, q).start()
-
-        relays(7.2 + 1.3 * q)
+        if q < CHUNKS - 1:
+            glue()
+        relays(7.2 + 1.4 * q)
     late(CHUNKS - 1)
-    relays(11.8)
     inv_rms = jnp.concatenate(inv_parts, axis=0)
 
     def projected(i, lo=0, hi=None):
         hi = rows if hi is None else hi
         a, b = spans[i]
         return (acc[lo:hi, a:b] * inv_rms[lo:hi]).astype(BF16)
-
-    def glue(lo, hi):
-        value = projected(2, lo, hi).astype(F32)
-        gate = projected(3, lo, hi).astype(F32)
-        return (value * jax.nn.sigmoid(gate)).astype(BF16)
-
-    tail_out[...] = glue(rows - PAD, rows)
-    tail = sp_copy(tail_out, tail_in, tail_sem.at[0], tail_sem.at[1], s + 1)
-
-    @pl.when(s + 1 < n_sp)
-    def _():
-        tail.start()
 
     query = projected(4).astype(F32) * (1.0 / math.sqrt(QK))
     heads = w_query.shape[1] // (2 * QK)
@@ -339,7 +377,7 @@
         for m in range(2):
             keep = (lane >= m * QK) & (lane < (m + 1) * QK)
             q4[2 * h + m] = jnp.where(keep, qh, 0.0).astype(BF16)
-    relays(12.6)
+    relays(11.9)
 
     key_pos = lax.broadcasted_iota(jnp.int32, (rows, rows), 0)
     query_pos = lax.broadcasted_iota(jnp.int32, (rows, rows), 1)
@@ -353,15 +391,17 @@
         m_ref[i] = tops[i]
         l_ref[i] = jnp.sum(exps[i], axis=0, keepdims=True)
         o_ref[i] = dot(v_own, exps[i].astype(BF16), 0, 0)
-    relays(13.6)
-
-    gl[PAD:, :] = glue(0, rows).astype(F32)
+    relays(12.7)
+
     gate_attn = projected(6).astype(F32)
     ga[...] = gate_attn * jax.nn.sigmoid(gate_attn)
 
     def visit(blocks, at=slice(None)):
         def stacked(plane):
-            parts = [kv[j, plane] for j in blocks]
+            parts = [
+                kv[b[0], plane, b[1] : b[2]] if isinstance(b, tuple) else kv[b, plane]
+                for b in blocks
+            ]
             return parts[0] if len(parts) == 1 else jnp.concatenate(parts, axis=0)
 
         k = stacked(0)
@@ -379,51 +419,69 @@
             l_ref[i, :, at] = l_ref[i, :, at] * factors[i] + jnp.sum(exps[i], axis=0, keepdims=True)
             o_ref[i, :, at] = o_ref[i, :, at] * factors[i] + news[i]
 
-    def mate_arrives(k):
-        for q in range(CHUNKS):
-            side(mate - 2 * k, q).wait_recv()
-
-    @pl.when(z >= 1)
-    def _():
-        visit([s - 2])
-
-    relays(14.8)
-
-    @pl.when(s == 0)
-    def _():
-        gl[:PAD, :] = jnp.zeros((PAD, gl.shape[1]), F32)
-
-    @pl.when(s > 0)
-    def _():
-        tail.wait_recv()
-        gl[:PAD, :] = tail_in[...].astype(F32)
-
-    n_taps = taps_ref.shape[0]
-    taps = taps_ref[...].astype(F32)
-    conv = jnp.zeros((rows, gl.shape[1]), F32)
-    for j in range(n_taps):
-        lo = PAD - (n_taps - 1) + j
-        conv = conv + gl[lo : lo + rows, :] * taps[j : j + 1, :]
-    ones = jnp.ones((8, conv.shape[1]), F32)
-    high = lax.Precision.HIGHEST
-    sq_out[...] = dot(ones, conv * conv, 1, 1, high)
-    gl[PAD:, :] = conv
+    middle = rows // 2
+
+    def mate_arrives(k, halves=(0, 1)):
+        for half in halves:
+            ref = kv.at[mate - 2 * k, :, half * middle : (half + 1) * middle, :]
+            sent(ref, side_recv.at[z - k, half])
+
     sq_copies = [
         tp_copy(sq_out, sq_in.at[i], sq_send.at[0], sq_recv.at[i], p)
         for i, p in enumerate((p1, p2, p3))
     ]
-    for copy in sq_copies:
-        copy.start()
-    relays(15.4)
-
+    high = lax.Precision.HIGHEST
+
+    def convolve():
+        @pl.when(s == 0)
+        def _():
+            gl[:PAD, :] = jnp.zeros((PAD, gl.shape[1]), F32)
+
+        @pl.when(s > 0)
+        def _():
+            tail.wait_recv()
+            gl[:PAD, :] = tail_in[...].astype(F32)
+
+        n_taps = taps_ref.shape[0]
+        taps = taps_ref[...].astype(F32)
+        conv = jnp.zeros((rows, gl.shape[1]), F32)
+        for j in range(n_taps):
+            lo = PAD - (n_taps - 1) + j
+            conv = conv + gl[lo : lo + rows, :] * taps[j : j + 1, :]
+        ones = jnp.ones((8, conv.shape[1]), F32)
+        sq_out[...] = dot(ones, conv * conv, 1, 1, high)
+        gl[PAD:, :] = conv
+        for copy in sq_copies:
+            copy.start()
     @pl.when(y == 1)
     def _():
+        convolve()
+
+    relays(13.6)
+
+    relays(14.0)
+
+    @pl.when(z >= 1)
+    def _():
+        visit([s - 2])
+
+    relays(15.3)
+
+    @pl.when(y == 0)
+    def _():
+        convolve()
+
+    relays(16.6)
+
+    @pl.when(y == 1)
+    def _():
         mate_arrives(0)
 
     @pl.when((y == 1) & (z > 0))
     def _():
         visit([mate])
 
+    conv_local = gl.shape[1]
     relays(100.0)
 
     if last_static >= 2:
@@ -447,11 +505,11 @@
     if nz - 1 > NEAR_STEPS:
         lax.fori_loop(NEAR_STEPS + 1, z + 1, beyond, 0)
 
+    conv_local = gl.shape[1]
     gate_conv = projected(5).astype(F32)
     for copy in sq_copies:
         copy.wait_recv()
     total_sq = sq_out[...] + sq_in[0] + sq_in[1] + sq_in[2]
-    conv_local = gl.shape[1]
     spread = jnp.full((8, conv_local), 0.125, F32)
     mean_sq = dot(total_sq, spread, 0, 0, high) / (conv_local * n_tp)
     normed = gl[PAD:, :] * lax.rsqrt(mean_sq + EPSILON) * conv_gain[...]
@@ -490,16 +548,26 @@
     def _():
         mate_arrives(1)
 
-    @pl.when(z >= 2)
-    def _():
-        visit([mate - 2])
-        mate_arrives(2)
+    if last_static >= 2:
+
+        @pl.when(z >= 2)
+        def _():
+            visit([mate - 2])
 
     if last_static >= 3:
 
         @pl.when(z >= 3)
         def _():
             mate_arrives(3)
+            visit([mate - 6])
+
+    if last_static >= 2:
+
+        @pl.when(z >= 2)
+        def _():
+            mate_arrives(2, (0,))
+            visit([(mate - 4, 0, middle)])
+            mate_arrives(2, (1,))
 
     def last_mate(at):
         @pl.when((z == 0) & (y == 1))
@@ -512,15 +580,9 @@
 
         if last_static >= 2:
 
-            @pl.when(z == 2)
+            @pl.when(z >= 2)
             def _():
-                visit([mate - 4], at)
-
-        if last_static >= 3:
-
-            @pl.when(z >= 3)
-            def _():
-                visit([mate - 4, mate - 6], at)
+                visit([(mate - 4, middle, rows)], at)
 
     last_mate(far_rows)
     finish(far_rows)
@@ -529,7 +591,7 @@
         return ybuf[pl.ds(pl.multiple_of(p * part, part), part), :]
 
     cols = w_out.shape[1] // PIECES
-    far = jnp.concatenate([block(p3), block(p2)], axis=0)
+    far = jnp.concatenate([block(p2), block(p3)], axis=0)
     a_copies = []
     for c in range(PIECES):
         r = dot(far, w_out[:, c * cols : (c + 1) * cols]).astype(BF16)
@@ -542,7 +604,7 @@
     for c in range(PIECES):
         a_copies[c].wait_recv()
         x_out[c] = (a_own[c].astype(F32) + a_in[c].astype(F32)).astype(BF16)
-        copy = tp_copy(x_out.at[c], x_in.at[c], x_sem.at[0], x_sem.at[1 + c], p2)
+        copy = tp_copy(x_out.at[c], x_in.at[c], x_sem.at[0], x_sem.at[1 + c], p3)
         copy.start()
         x_copies.append(copy)
     last_mate(near_rows)
@@ -556,9 +618,6 @@
         copy = tp_copy(b_out.at[c], b_in.at[c], b_sem.at[0], b_sem.at[1 + c], p1)
         copy.start()
         b_copies.append(copy)
-    def sent(ref, sem):
-        pltpu.make_async_copy(ref, ref, sem).wait()
-
     sent(tok, tok_send.at[0])
     sent(tok, tok_send.at[1])
     sent(tok, tok_send.at[2])
@@ -571,7 +630,7 @@
 
     @pl.when(has_up)
     def _():
-        sent(kv.at[s], up_send.at[s])
+        sent(kv.at[s], up_send.at[z])
 
     @pl.when(has_skip)
     def _():
@@ -579,16 +638,16 @@
 
     @pl.when(y == 0)
     def _():
-        sent(kv.at[s], side_send.at[s])
+        sent(kv.at[s], side_send.at[z])
 
     def drain(k, carry):
         j = s - 2 * k
 
         @pl.when(has_up & (k != SKIP - 1))
         def _():
-            sent(kv.at[j], up_send.at[j])
-
-        sent(kv.at[j], side_send.at[j])
+            sent(kv.at[j], up_send.at[z - k])
+
+        sent(kv.at[j], side_send.at[z - k])
         return carry
 
     lax.fori_loop(1, z + 1, drain, 0)
@@ -646,10 +705,11 @@
             dma((2,)),
             dma((3,)),
             dma((2 * CHUNKS + 1,)),
-            dma((n_sp, CHUNKS)),
-            dma((n_sp,)),
+            dma((n_sp // 2, CHUNKS)),
+            dma((n_sp // 2, 2)),
+            dma((n_sp // 2,)),
             dma((1,)),
-            dma((n_sp,)),
+            dma((n_sp // 2,)),
             dma((2,)),
             dma((1,)),
             dma((3,)),
@@ -665,6 +725,8 @@
             pltpu.VMEM((1, VDIM), F32),
             pltpu.VMEM((rows, heads * VDIM), F32),
             dma((6,)),
+            pltpu.SemaphoreType.REGULAR,
+            pltpu.SemaphoreType.REGULAR,
         ],
         compiler_params=pltpu.CompilerParams(
             collective_id=0, has_side_effects=True, vmem_limit_bytes=60 * 1024 * 1024

time: 34.3 us -> 33 us (0.962)
  Pallas kernels: 33.4 us -> 32.2 us
    pallas_call x1, Pallas kernels: 33.4 us -> 32.2 us  [local(): pl.pallas_call(functools.partial(kernel, n_sp, n_tp), out_shape=pltpu.VME...]
where the time goes in v2:
time: 33 us; the launch traced here: 32.9 us
  Pallas kernels  32.2 us (98%)
  local copies, waits for them, and re-layouts  0.71 us (2%)
    pallas_call x1, Pallas kernels, local(): pl.pallas_call(functools.partial(kernel, n_sp, n_tp), out_shape=pltpu.VME...  32.2 us
    unnamed x1, local copies, waits for them, and re-layouts  0.71 us

profile of v2, /device:TPU:25, one launch (start us, length us, event | category | flops | bytes accessed | tf_op | source)
XLA Modules:
  0.0 32.9 jit_solution(2456047423644226282)
XLA Ops:
  0.0 32.2 %shard_map.145 = bf16[64,2048]{1,0:T(8,128)(2,1)S(1)} custom-call(bf16[256,512]{1,0:T(8,128)(2,1)} %tok_hbm.1, bf16[16,128]{1,0:T(8,128)(2,1)} %bitcast.4, bf16[2048,128]{1,0:T(8,128)(2,1)} %w_glu_value.1, bf16[2048,128]{1,0:T(8,128)(2,1)} %w_glu_gate.1, bf16[2048,256]{1,0:T(8,128)(2,1)} %w_query.1, bf16[2048,128]{1,0:T(8,128)(2,1)} %w_key.1, ...), custom_call_target="tpu_custom_call" | custom-call | tf_op jit(solution)/shard_map/pallas_call | solution.py:682
  32.2 0.7 %copy.17 = bf16[64,2048]{1,0:T(8,128)(2,1)} copy(bf16[64,2048]{1,0:T(8,128)(2,1)S(1)} %shard_map.145) | data formatting | bytes 524288

commit v3 on v2

--- a/solution.py
+++ b/solution.py
@@ -17,6 +17,7 @@
 F32 = jnp.float32
 BF16 = jnp.bfloat16
 PIECES = 4
+LEAD = 256
 PAD = 32
 LANES = 128
 CHUNKS = 4
@@ -74,6 +75,8 @@
     b_out,
     b_own,
     b_in,
+    d_out,
+    d_in,
     w_sem,
     tok_send,
     tok_recv,
@@ -88,6 +91,7 @@
     a_sem,
     x_sem,
     b_sem,
+    d_sem,
     gain32,
     tok,
     gain,
@@ -193,9 +197,14 @@
         for q in range(CHUNKS)
     ]
     beside = tp_copy(tok, tokbuf.at[0], tok_send.at[2], tok_recv.at[2 * CHUNKS], p1)
-    for copy in across:
-        copy.start()
+    across[0].start()
     beside.start()
+
+    @pl.when(core == 0)
+    def _():
+        for copy in across[1:]:
+            copy.start()
+
     for copy in out_loads:
         copy.start()
 
@@ -236,6 +245,12 @@
         tell(far_sem)
 
     pltpu.make_async_copy(w_all, w_all, w_sem.at[0]).wait()
+
+    @pl.when(core == 1)
+    def _():
+        for copy in across[1:]:
+            copy.start()
+
     beside.wait_recv()
     scaled, more = prepare(tokbuf[0], p1)
     squares = squares + more
@@ -283,7 +298,7 @@
 
     def due(steps, k, q):
         if k == 1:
-            return 9.9 + 1.3 * q
+            return 9.9 + 1.43 * q
         return 11.3 + 1.3 * q if k == SKIP else 14.9 + 0.7 * q
 
     pending = {
@@ -293,6 +308,9 @@
         )
         for steps in range(1, last_static + 1)
     }
+
+    for queue in pending.values():
+        queue.remove((1, 0))
 
     def relays(until):
         for steps, queue in pending.items():
@@ -359,6 +377,18 @@
 
         if q < CHUNKS - 1:
             glue()
+        if q == CHUNKS - 2:
+
+            @pl.when((z >= 1) & (core == 1))
+            def _():
+                relay(1, 0)
+
+        if q == CHUNKS - 1:
+
+            @pl.when((z >= 1) & (core == 0))
+            def _():
+                relay(1, 0)
+
         relays(7.2 + 1.4 * q)
     late(CHUNKS - 1)
     inv_rms = jnp.concatenate(inv_parts, axis=0)
@@ -391,7 +421,7 @@
         m_ref[i] = tops[i]
         l_ref[i] = jnp.sum(exps[i], axis=0, keepdims=True)
         o_ref[i] = dot(v_own, exps[i].astype(BF16), 0, 0)
-    relays(12.7)
+    relays(12.8)
 
     gate_attn = projected(6).astype(F32)
     ga[...] = gate_attn * jax.nn.sigmoid(gate_attn)
@@ -457,9 +487,9 @@
     def _():
         convolve()
 
-    relays(13.6)
-
-    relays(14.0)
+    relays(14.01)
+
+    relays(15.25)
 
     @pl.when(z >= 1)
     def _():
@@ -590,39 +620,52 @@
     def block(p):
         return ybuf[pl.ds(pl.multiple_of(p * part, part), part), :]
 
-    cols = w_out.shape[1] // PIECES
+    width_out = w_out.shape[1]
+    lanes = (width_out - LEAD) // LANES
+    edges = [LEAD + LANES * (lanes * c // PIECES) for c in range(PIECES + 1)]
+    ranges = [slice(lo, hi) for lo, hi in zip(edges, edges[1:])]
+    lead = slice(0, LEAD)
     far = jnp.concatenate([block(p2), block(p3)], axis=0)
+    r = dot(far, w_out[:, lead]).astype(BF16)
+    x_out[:, lead] = r[part:]
+    d_out[...] = r[:part]
+    direct = [
+        tp_copy(x_out.at[:, lead], x_in.at[:, lead], x_sem.at[1], x_sem.at[2], p3),
+        tp_copy(d_out, d_in, d_sem.at[0], d_sem.at[1], p2),
+    ]
+    for copy in direct:
+        copy.start()
     a_copies = []
-    for c in range(PIECES):
-        r = dot(far, w_out[:, c * cols : (c + 1) * cols]).astype(BF16)
-        a_out[c] = r[:part]
-        a_own[c] = r[part:]
-        copy = tp_copy(a_out.at[c], a_in.at[c], a_sem.at[0], a_sem.at[1 + c], p1)
+    for c, at in enumerate(ranges):
+        r = dot(far, w_out[:, at]).astype(BF16)
+        a_out[:, at] = r[:part]
+        a_own[:, at] = r[part:]
+        copy = tp_copy(a_out.at[:, at], a_in.at[:, at], a_sem.at[0], a_sem.at[1 + c], p1)
         copy.start()
         a_copies.append(copy)
     x_copies = []
-    for c in range(PIECES):
+    for c, at in enumerate(ranges):
         a_copies[c].wait_recv()
-        x_out[c] = (a_own[c].astype(F32) + a_in[c].astype(F32)).astype(BF16)
-        copy = tp_copy(x_out.at[c], x_in.at[c], x_sem.at[0], x_sem.at[1 + c], p3)
+        x_out[:, at] = (a_own[:, at].astype(F32) + a_in[:, at].astype(F32)).astype(BF16)
+        copy = tp_copy(x_out.at[:, at], x_in.at[:, at], x_sem.at[0], x_sem.at[3 + c], p3)
         copy.start()
         x_copies.append(copy)
     last_mate(near_rows)
     finish(near_rows)
     near = jnp.concatenate([block(p1), block(t)], axis=0)
-    b_copies = []
-    for c in range(PIECES):
-        r = dot(near, w_out[:, c * cols : (c + 1) * cols]).astype(BF16)
-        b_out[c] = r[:part]
-        b_own[c] = r[part:]
-        copy = tp_copy(b_out.at[c], b_in.at[c], b_sem.at[0], b_sem.at[1 + c], p1)
-        copy.start()
-        b_copies.append(copy)
+    half_out = width_out // 2
+    for c in range(2):
+        at = slice(c * half_out, (c + 1) * half_out)
+        r = dot(near, w_out[:, at]).astype(BF16)
+        b_out[:, at] = r[:part]
+        b_own[:, at] = r[part:].astype(F32)
+    b_copy = tp_copy(b_out, b_in, b_sem.at[0], b_sem.at[1], p1)
+    b_copy.start()
     sent(tok, tok_send.at[0])
     sent(tok, tok_send.at[1])
     sent(tok, tok_send.at[2])
     sent(sq_in, sq_send.at[0])
-    sent(a_out, a_sem.at[0])
+    sent(a_out.at[:, LEAD:], a_sem.at[0])
 
     @pl.when(s + 1 < n_sp)
     def _():
@@ -651,14 +694,19 @@
         return carry
 
     lax.fori_loop(1, z + 1, drain, 0)
-    for c in range(PIECES):
-        b_copies[c].wait_recv()
-    for c in range(PIECES):
+    b_copy.wait_recv()
+    b_own[...] = (b_own[...].astype(F32) + b_in[...].astype(F32))
+    for copy in direct:
+        copy.wait_recv()
+    out[:, lead] = (
+        b_own[:, lead] + x_in[:, lead].astype(F32) + d_in[...].astype(F32)
+    ).astype(BF16)
+    for c, at in enumerate(ranges):
         x_copies[c].wait_recv()
-        out[:, c * cols : (c + 1) * cols] = (
-            b_own[c].astype(F32) + b_in[c].astype(F32) + x_in[c].astype(F32)
-        ).astype(BF16)
-    sent(x_out, x_sem.at[0])
+        out[:, at] = (b_own[:, at] + x_in[:, at].astype(F32)).astype(BF16)
+    for copy in direct:
+        copy.wait_send()
+    sent(x_out.at[:, LEAD:], x_sem.at[0])
     sent(b_out, b_sem.at[0])
 
 
@@ -674,11 +722,10 @@
     conv_local = conv_weight.shape[1]
     heads = lam.shape[0]
     part = rows // n_tp
-    cols = out_cols // PIECES
     vmem = pl.BlockSpec(memory_space=pltpu.VMEM)
     hbm = pl.BlockSpec(memory_space=pl.ANY)
     dma = pltpu.SemaphoreType.DMA
-    piece = pltpu.VMEM((PIECES, part, cols), BF16)
+    piece = pltpu.VMEM((part, out_cols), BF16)
     return pl.pallas_call(
         functools.partial(kernel, n_sp, n_tp),
         out_shape=pltpu.VMEM((part, out_cols), BF16),
@@ -701,11 +748,15 @@
             pltpu.VMEM((8, rows), F32),
             pltpu.VMEM((3, 8, rows), F32),
             pltpu.VMEM((rows, out_rows), BF16),
-            piece, piece, piece, piece, piece, piece, piece, piece,
+            piece, piece, piece, piece, piece, piece,
+            pltpu.VMEM((part, out_cols), F32),
+            piece,
+            pltpu.VMEM((part, LEAD), BF16),
+            pltpu.VMEM((part, LEAD), BF16),
             dma((2,)),
             dma((3,)),
             dma((2 * CHUNKS + 1,)),
-            dma((n_sp // 2, CHUNKS)),
+            dma((max(n_sp // 2 - 1, 1), CHUNKS)),
             dma((n_sp // 2, 2)),
             dma((n_sp // 2,)),
             dma((1,)),
@@ -714,8 +765,9 @@
             dma((1,)),
             dma((3,)),
             dma((1 + PIECES,)),
-            dma((1 + PIECES,)),
-            dma((1 + PIECES,)),
+            dma((3 + PIECES,)),
+            dma((2,)),
+            dma((2,)),
             pltpu.VMEM((width // LANES, LANES), F32),
             pltpu.VMEM(tokens.shape, BF16),
             pltpu.VMEM((width // LANES, LANES), BF16),

time: 33 us -> 31.9 us (0.967)
  Pallas kernels: 32.2 us -> 31.1 us
    pallas_call x1, Pallas kernels: 32.2 us -> 31.1 us  [local(): pl.pallas_call(functools.partial(kernel, n_sp, n_tp), out_shape=pltpu.VME...]
where the time goes in v3:
time: 31.9 us; the launch traced here: 31.8 us
  Pallas kernels  31.1 us (97%)
  local copies, waits for them, and re-layouts  0.71 us (2%)
    pallas_call x1, Pallas kernels, local(): pl.pallas_call(functools.partial(kernel, n_sp, n_tp), out_shape=pltpu.VME...  31.1 us
    unnamed x1, local copies, waits for them, and re-layouts  0.71 us

profile of v3, /device:TPU:25, one launch (start us, length us, event | category | flops | bytes accessed | tf_op | source)
XLA Modules:
  0.0 31.8 jit_solution(1385818085729987010)
XLA Ops:
  0.0 31.1 %shard_map.145 = bf16[64,2048]{1,0:T(8,128)(2,1)S(1)} custom-call(bf16[256,512]{1,0:T(8,128)(2,1)} %tok_hbm.1, bf16[16,128]{1,0:T(8,128)(2,1)} %bitcast.4, bf16[2048,128]{1,0:T(8,128)(2,1)} %w_glu_value.1, bf16[2048,128]{1,0:T(8,128)(2,1)} %w_glu_gate.1, bf16[2048,256]{1,0:T(8,128)(2,1)} %w_query.1, bf16[2048,128]{1,0:T(8,128)(2,1)} %w_key.1, ...), custom_call_target="tpu_custom_call" | custom-call | tf_op jit(solution)/shard_map/pallas_call | solution.py:729
  31.1 0.7 %copy.17 = bf16[64,2048]{1,0:T(8,128)(2,1)} copy(bf16[64,2048]{1,0:T(8,128)(2,1)S(1)} %shard_map.145) | data formatting | bytes 524288

commit v4 on v3

--- a/solution.py
+++ b/solution.py
@@ -16,8 +16,8 @@
 MESH = pl.DeviceIdType.MESH
 F32 = jnp.float32
 BF16 = jnp.bfloat16
-PIECES = 4
-LEAD = 256
+PIECES = 3
+GATHER = 256
 PAD = 32
 LANES = 128
 CHUNKS = 4
@@ -75,8 +75,10 @@
     b_out,
     b_own,
     b_in,
-    d_out,
-    d_in,
+    wf,
+    yg,
+    e_out,
+    e_in,
     w_sem,
     tok_send,
     tok_recv,
@@ -91,7 +93,8 @@
     a_sem,
     x_sem,
     b_sem,
-    d_sem,
+    g_send,
+    g_recv,
     gain32,
     tok,
     gain,
@@ -391,6 +394,18 @@
 
         relays(7.2 + 1.4 * q)
     late(CHUNKS - 1)
+    sent(w_out, w_sem.at[1])
+    shared = w_out.shape[1] - 2 * GATHER
+
+    def gather_cols(parity):
+        return pl.ds(pl.multiple_of(shared + parity * GATHER, GATHER), GATHER)
+
+    w_copies = [
+        tp_copy(w_out.at[:, gather_cols(parity)], wf.at[i], g_send.at[i], g_recv.at[i], p)
+        for i, (p, parity) in enumerate(((p1, 1 - core), (p2, core), (p3, 1 - core)))
+    ]
+    w_copies[0].start()
+    w_copies[1].start()
     inv_rms = jnp.concatenate(inv_parts, axis=0)
 
     def projected(i, lo=0, hi=None):
@@ -483,6 +498,7 @@
         gl[PAD:, :] = conv
         for copy in sq_copies:
             copy.start()
+        w_copies[2].start()
     @pl.when(y == 1)
     def _():
         convolve()
@@ -495,7 +511,7 @@
     def _():
         visit([s - 2])
 
-    relays(15.3)
+    relays(15.65)
 
     @pl.when(y == 0)
     def _():
@@ -551,6 +567,13 @@
     both = 2 * part
     far_rows = pl.ds(pl.multiple_of(p2 // 2 * both, both), both)
     near_rows = pl.ds(pl.multiple_of(t // 2 * both, both), both)
+    yc_copy = tp_copy(
+        ybuf.at[far_rows, :conv_local], yg.at[1, :, :conv_local], g_send.at[3], g_recv.at[3], p3
+    )
+    ya_copy = tp_copy(
+        ybuf.at[far_rows, conv_local:], yg.at[1, :, conv_local:], g_send.at[4], g_recv.at[4], p3
+    )
+    yc_copy.start()
 
     def finish(at):
         for h in range(heads):
@@ -564,8 +587,6 @@
                 n * ga[at, lo : lo + VDIM]
             ).astype(BF16)
 
-    pltpu.make_async_copy(w_out, w_out, w_sem.at[1]).wait()
-
     def beyond_mate(k, carry):
         mate_arrives(k)
         visit([mate - 2 * k])
@@ -620,21 +641,11 @@
     def block(p):
         return ybuf[pl.ds(pl.multiple_of(p * part, part), part), :]
 
-    width_out = w_out.shape[1]
-    lanes = (width_out - LEAD) // LANES
-    edges = [LEAD + LANES * (lanes * c // PIECES) for c in range(PIECES + 1)]
+    ya_copy.start()
+    lanes = shared // LANES
+    edges = [LANES * (lanes * c // PIECES) for c in range(PIECES + 1)]
     ranges = [slice(lo, hi) for lo, hi in zip(edges, edges[1:])]
-    lead = slice(0, LEAD)
     far = jnp.concatenate([block(p2), block(p3)], axis=0)
-    r = dot(far, w_out[:, lead]).astype(BF16)
-    x_out[:, lead] = r[part:]
-    d_out[...] = r[:part]
-    direct = [
-        tp_copy(x_out.at[:, lead], x_in.at[:, lead], x_sem.at[1], x_sem.at[2], p3),
-        tp_copy(d_out, d_in, d_sem.at[0], d_sem.at[1], p2),
-    ]
-    for copy in direct:
-        copy.start()
     a_copies = []
     for c, at in enumerate(ranges):
         r = dot(far, w_out[:, at]).astype(BF16)
@@ -647,25 +658,42 @@
     for c, at in enumerate(ranges):
         a_copies[c].wait_recv()
         x_out[:, at] = (a_own[:, at].astype(F32) + a_in[:, at].astype(F32)).astype(BF16)
-        copy = tp_copy(x_out.at[:, at], x_in.at[:, at], x_sem.at[0], x_sem.at[3 + c], p3)
+        copy = tp_copy(x_out.at[:, at], x_in.at[:, at], x_sem.at[0], x_sem.at[1 + c], p3)
         copy.start()
         x_copies.append(copy)
     last_mate(near_rows)
     finish(near_rows)
+    yn_copy = tp_copy(ybuf.at[near_rows, :], yg.at[0], g_send.at[5], g_recv.at[5], p1)
+    yn_copy.start()
     near = jnp.concatenate([block(p1), block(t)], axis=0)
-    half_out = width_out // 2
     for c in range(2):
-        at = slice(c * half_out, (c + 1) * half_out)
+        at = slice(c * (shared // 2), (c + 1) * (shared // 2))
         r = dot(near, w_out[:, at]).astype(BF16)
         b_out[:, at] = r[:part]
         b_own[:, at] = r[part:].astype(F32)
     b_copy = tp_copy(b_out, b_in, b_sem.at[0], b_sem.at[1], p1)
     b_copy.start()
+    yc_copy.wait_recv()
+    ya_copy.wait_recv()
+    pass_copy = tp_copy(yg.at[1], yg.at[2], g_send.at[6], g_recv.at[6], p1)
+    pass_copy.start()
+    for copy in w_copies:
+        copy.wait_recv()
+    yn_copy.wait_recv()
+    whole = dot(ybuf[near_rows, :], w_out[:, gather_cols(core)])
+    whole = whole + dot(yg[0], wf[0]) + dot(yg[1], wf[2])
+    pass_copy.wait_recv()
+    e_out[...] = (whole + dot(yg[2], wf[1])).astype(BF16)
+    e_copy = tp_copy(
+        e_out.at[pl.ds(pl.multiple_of((1 - core) * part, part), part)], e_in,
+        g_send.at[7], g_recv.at[7], p1,
+    )
+    e_copy.start()
     sent(tok, tok_send.at[0])
     sent(tok, tok_send.at[1])
     sent(tok, tok_send.at[2])
     sent(sq_in, sq_send.at[0])
-    sent(a_out.at[:, LEAD:], a_sem.at[0])
+    sent(a_out, a_sem.at[0])
 
     @pl.when(s + 1 < n_sp)
     def _():
@@ -695,18 +723,16 @@
 
     lax.fori_loop(1, z + 1, drain, 0)
     b_copy.wait_recv()
-    b_own[...] = (b_own[...].astype(F32) + b_in[...].astype(F32))
-    for copy in direct:
-        copy.wait_recv()
-    out[:, lead] = (
-        b_own[:, lead] + x_in[:, lead].astype(F32) + d_in[...].astype(F32)
-    ).astype(BF16)
+    b_own[...] = b_own[...] + b_in[...].astype(F32)
+    e_copy.wait_recv()
+    out[:, gather_cols(core)] = e_out[pl.ds(pl.multiple_of(core * part, part), part), :]
+    out[:, gather_cols(1 - core)] = e_in[...]
+    for copy in w_copies + [yc_copy, ya_copy, yn_copy, pass_copy, e_copy]:
+        copy.wait_send()
     for c, at in enumerate(ranges):
         x_copies[c].wait_recv()
         out[:, at] = (b_own[:, at] + x_in[:, at].astype(F32)).astype(BF16)
-    for copy in direct:
-        copy.wait_send()
-    sent(x_out.at[:, LEAD:], x_sem.at[0])
+    sent(x_out, x_sem.at[0])
     sent(b_out, b_sem.at[0])
 
 
@@ -725,7 +751,8 @@
     vmem = pl.BlockSpec(memory_space=pltpu.VMEM)
     hbm = pl.BlockSpec(memory_space=pl.ANY)
     dma = pltpu.SemaphoreType.DMA
-    piece = pltpu.VMEM((part, out_cols), BF16)
+    shared = out_cols - 2 * GATHER
+    piece = pltpu.VMEM((part, shared), BF16)
     return pl.pallas_call(
         functools.partial(kernel, n_sp, n_tp),
         out_shape=pltpu.VMEM((part, out_cols), BF16),
@@ -749,10 +776,12 @@
             pltpu.VMEM((3, 8, rows), F32),
             pltpu.VMEM((rows, out_rows), BF16),
             piece, piece, piece, piece, piece, piece,
-            pltpu.VMEM((part, out_cols), F32),
+            pltpu.VMEM((part, shared), F32),
             piece,
-            pltpu.VMEM((part, LEAD), BF16),
-            pltpu.VMEM((part, LEAD), BF16),
+            pltpu.VMEM((3, out_rows, GATHER), BF16),
+            pltpu.VMEM((3, 2 * part, out_rows), BF16),
+            pltpu.VMEM((2 * part, GATHER), BF16),
+            pltpu.VMEM((part, GATHER), BF16),
             dma((2,)),
             dma((3,)),
             dma((2 * CHUNKS + 1,)),
@@ -765,9 +794,10 @@
             dma((1,)),
             dma((3,)),
             dma((1 + PIECES,)),
-            dma((3 + PIECES,)),
+            dma((1 + PIECES,)),
             dma((2,)),
-            dma((2,)),
+            dma((8,)),
+            dma((8,)),
             pltpu.VMEM((width // LANES, LANES), F32),
             pltpu.VMEM(tokens.shape, BF16),
             pltpu.VMEM((width // LANES, LANES), BF16),

time: 31.9 us -> 31.2 us (0.978)
  Pallas kernels: 31.1 us -> 30.3 us
    pallas_call x1, Pallas kernels: 31.1 us -> 30.3 us  [local(): pl.pallas_call(functools.partial(kernel, n_sp, n_tp), out_shape=pltpu.VME...]
where the time goes in v4:
time: 31.2 us; the launch traced here: 31 us
  Pallas kernels  30.3 us (97%)
  local copies, waits for them, and re-layouts  0.71 us (2%)
    pallas_call x1, Pallas kernels, local(): pl.pallas_call(functools.partial(kernel, n_sp, n_tp), out_shape=pltpu.VME...  30.3 us
    unnamed x1, local copies, waits for them, and re-layouts  0.71 us

profile of v4, /device:TPU:25, one launch (start us, length us, event | category | flops | bytes accessed | tf_op | source)
XLA Modules:
  0.0 31.0 jit_solution(11341514943877536545)
XLA Ops:
  0.0 30.3 %shard_map.145 = bf16[64,2048]{1,0:T(8,128)(2,1)S(1)} custom-call(bf16[256,512]{1,0:T(8,128)(2,1)} %tok_hbm.1, bf16[16,128]{1,0:T(8,128)(2,1)} %bitcast.4, bf16[2048,128]{1,0:T(8,128)(2,1)} %w_glu_value.1, bf16[2048,128]{1,0:T(8,128)(2,1)} %w_glu_gate.1, bf16[2048,256]{1,0:T(8,128)(2,1)} %w_query.1, bf16[2048,128]{1,0:T(8,128)(2,1)} %w_key.1, ...), custom_call_target="tpu_custom_call" | custom-call | tf_op jit(solution)/shard_map/pallas_call | solution.py:756
  30.3 0.7 %copy.17 = bf16[64,2048]{1,0:T(8,128)(2,1)} copy(bf16[64,2048]{1,0:T(8,128)(2,1)S(1)} %shard_map.145) | data formatting | bytes 524288

commit v5 on v4

--- a/solution.py
+++ b/solution.py
@@ -195,11 +195,11 @@
     passed = [
         tp_copy(
             tokbuf.at[1, piece_rows(q)], tokbuf.at[2, piece_rows(q)],
-            tok_send.at[1], tok_recv.at[CHUNKS + q], p1,
+            tok_send.at[0], tok_recv.at[CHUNKS + q], p1,
         )
         for q in range(CHUNKS)
     ]
-    beside = tp_copy(tok, tokbuf.at[0], tok_send.at[2], tok_recv.at[2 * CHUNKS], p1)
+    beside = tp_copy(tok, tokbuf.at[0], tok_send.at[0], tok_recv.at[2 * CHUNKS], p1)
     across[0].start()
     beside.start()
 
@@ -401,7 +401,7 @@
         return pl.ds(pl.multiple_of(shared + parity * GATHER, GATHER), GATHER)
 
     w_copies = [
-        tp_copy(w_out.at[:, gather_cols(parity)], wf.at[i], g_send.at[i], g_recv.at[i], p)
+        tp_copy(w_out.at[:, gather_cols(parity)], wf.at[i], g_send.at[0], g_recv.at[0], p)
         for i, (p, parity) in enumerate(((p1, 1 - core), (p2, core), (p3, 1 - core)))
     ]
     w_copies[0].start()
@@ -568,10 +568,10 @@
     far_rows = pl.ds(pl.multiple_of(p2 // 2 * both, both), both)
     near_rows = pl.ds(pl.multiple_of(t // 2 * both, both), both)
     yc_copy = tp_copy(
-        ybuf.at[far_rows, :conv_local], yg.at[1, :, :conv_local], g_send.at[3], g_recv.at[3], p3
+        ybuf.at[far_rows, :conv_local], yg.at[1, :, :conv_local], g_send.at[1], g_recv.at[1], p3
     )
     ya_copy = tp_copy(
-        ybuf.at[far_rows, conv_local:], yg.at[1, :, conv_local:], g_send.at[4], g_recv.at[4], p3
+        ybuf.at[far_rows, conv_local:], yg.at[1, :, conv_local:], g_send.at[1], g_recv.at[1], p3
     )
     yc_copy.start()
 
@@ -663,7 +663,7 @@
         x_copies.append(copy)
     last_mate(near_rows)
     finish(near_rows)
-    yn_copy = tp_copy(ybuf.at[near_rows, :], yg.at[0], g_send.at[5], g_recv.at[5], p1)
+    yn_copy = tp_copy(ybuf.at[near_rows, :], yg.at[0], g_send.at[2], g_recv.at[2], p1)
     yn_copy.start()
     near = jnp.concatenate([block(p1), block(t)], axis=0)
     for c in range(2):
@@ -673,12 +673,10 @@
         b_own[:, at] = r[part:].astype(F32)
     b_copy = tp_copy(b_out, b_in, b_sem.at[0], b_sem.at[1], p1)
     b_copy.start()
-    yc_copy.wait_recv()
-    ya_copy.wait_recv()
-    pass_copy = tp_copy(yg.at[1], yg.at[2], g_send.at[6], g_recv.at[6], p1)
+    sent(yg.at[1], g_recv.at[1])
+    pass_copy = tp_copy(yg.at[1], yg.at[2], g_send.at[3], g_recv.at[3], p1)
     pass_copy.start()
-    for copy in w_copies:
-        copy.wait_recv()
+    sent(wf, g_recv.at[0])
     yn_copy.wait_recv()
     whole = dot(ybuf[near_rows, :], w_out[:, gather_cols(core)])
     whole = whole + dot(yg[0], wf[0]) + dot(yg[1], wf[2])
@@ -686,12 +684,10 @@
     e_out[...] = (whole + dot(yg[2], wf[1])).astype(BF16)
     e_copy = tp_copy(
         e_out.at[pl.ds(pl.multiple_of((1 - core) * part, part), part)], e_in,
-        g_send.at[7], g_recv.at[7], p1,
+        g_send.at[4], g_recv.at[4], p1,
     )
     e_copy.start()
-    sent(tok, tok_send.at[0])
-    sent(tok, tok_send.at[1])
-    sent(tok, tok_send.at[2])
+    sent(tokbuf, tok_send.at[0])
     sent(sq_in, sq_send.at[0])
     sent(a_out, a_sem.at[0])
 
@@ -727,7 +723,9 @@
     e_copy.wait_recv()
     out[:, gather_cols(core)] = e_out[pl.ds(pl.multiple_of(core * part, part), part), :]
     out[:, gather_cols(1 - core)] = e_in[...]
-    for copy in w_copies + [yc_copy, ya_copy, yn_copy, pass_copy, e_copy]:
+    sent(wf, g_send.at[0])
+    sent(yg.at[1], g_send.at[1])
+    for copy in (yn_copy, pass_copy, e_copy):
         copy.wait_send()
     for c, at in enumerate(ranges):
         x_copies[c].wait_recv()
@@ -783,7 +781,7 @@
             pltpu.VMEM((2 * part, GATHER), BF16),
             pltpu.VMEM((part, GATHER), BF16),
             dma((2,)),
-            dma((3,)),
+            dma((1,)),
             dma((2 * CHUNKS + 1,)),
             dma((max(n_sp // 2 - 1, 1), CHUNKS)),
             dma((n_sp // 2, 2)),
@@ -796,8 +794,8 @@
             dma((1 + PIECES,)),
             dma((1 + PIECES,)),
             dma((2,)),
-            dma((8,)),
-            dma((8,)),
+            dma((5,)),
+            dma((5,)),
             pltpu.VMEM((width // LANES, LANES), F32),
             pltpu.VMEM(tokens.shape, BF16),
             pltpu.VMEM((width // LANES, LANES), BF16),

time: 31.2 us -> 31.1 us (level)
  no operation moved by 1% of the time
where the time goes in v5:
time: 31.1 us; the launch traced here: 30.9 us
  Pallas kernels  30.2 us (97%)
  local copies, waits for them, and re-layouts  0.71 us (2%)
    pallas_call x1, Pallas kernels, local(): pl.pallas_call(functools.partial(kernel, n_sp, n_tp), out_shape=pltpu.VME...  30.2 us
    unnamed x1, local copies, waits for them, and re-layouts  0.71 us

profile of v5, /device:TPU:25, one launch (start us, length us, event | category | flops | bytes accessed | tf_op | source)
XLA Modules:
  0.0 30.9 jit_solution(17503327921748347685)
XLA Ops:
  0.0 30.2 %shard_map.145 = bf16[64,2048]{1,0:T(8,128)(2,1)S(1)} custom-call(bf16[256,512]{1,0:T(8,128)(2,1)} %tok_hbm.1, bf16[16,128]{1,0:T(8,128)(2,1)} %bitcast.4, bf16[2048,128]{1,0:T(8,128)(2,1)} %w_glu_value.1, bf16[2048,128]{1,0:T(8,128)(2,1)} %w_glu_gate.1, bf16[2048,256]{1,0:T(8,128)(2,1)} %w_query.1, bf16[2048,128]{1,0:T(8,128)(2,1)} %w_key.1, ...), custom_call_target="tpu_custom_call" | custom-call | tf_op jit(solution)/shard_map/pallas_call | solution.py:754
  30.2 0.7 %copy.17 = bf16[64,2048]{1,0:T(8,128)(2,1)} copy(bf16[64,2048]{1,0:T(8,128)(2,1)S(1)} %shard_map.145) | data formatting | bytes 524288
